TPU v7x, 32 devices: a whole 2x2x4 slice. The times are simulated.
32 devices in a mesh: sp: 16 (over z, y, x), tp: 2 (over core).
Axes of the slice: x: 2, y: 2, z: 4, core: 2. Of those that a mesh axis runs over, the one named last changes fastest.
Arguments:
- tokens: bfloat16 [1536, 4, 1024], P(('sp', 'tp')), may hold values from -6 to 6
- in_gain: float32 [1024], replicated, may hold values from 0.1 to 1.9
- w_query: bfloat16 [1024, 1024], P('sp', 'tp'), may hold values from -0.1875 to 0.1875
- w_key: bfloat16 [1024, 1024], P('sp', 'tp'), may hold values from -0.1875 to 0.1875
- w_value: bfloat16 [1024, 1024], P('sp', 'tp'), may hold values from -0.1875 to 0.1875
- w_gate: bfloat16 [1024, 1024], P('sp', 'tp'), may hold values from -0.1875 to 0.1875
- w_beta: bfloat16 [1024, 8], P('sp', 'tp'), may hold values from -0.1875 to 0.1875
- conv_query: bfloat16 [4, 1024], P(None, 'tp'), may hold values from -3 to 3
- conv_key: bfloat16 [4, 1024], P(None, 'tp'), may hold values from -3 to 3
- conv_value: bfloat16 [4, 1024], P(None, 'tp'), may hold values from -3 to 3
- decay_rate: float32 [8], P('tp'), may hold values from 0.1 to 3
- out_gain: float32 [128], replicated, may hold values from 0.1 to 1.9
- w_out: bfloat16 [1024, 1024], P('tp', 'sp'), may hold values from -0.1875 to 0.1875
Outputs:
- mixed: bfloat16 [1536, 4, 1024], P(('sp', 'tp'))
All inputs are finite; a program needn't handle non-finite values.
Results may differ from a plain program's by a relative error of at most 0.02.
Values may be sent and summed in bfloat16 or wider, within the bound.
A program may use at most 64 MiB of HBM per device.

v0:
```python
import math

import jax
import jax.numpy as jnp
from jax import lax
from jax.sharding import PartitionSpec as P

BLOCK = 32


epsilon = 1e-06
out_epsilon = 1e-10
highest = lax.Precision.HIGHEST


def on_whole(piece, axis, dim, apply):
    everything = lax.all_gather(piece, axis, axis=dim, tiled=True)
    return apply(everything, jnp.int32(0))


def for_sending(x):
    return jax.tree.map(lambda a: a.astype(jnp.bfloat16) if a.dtype == jnp.float32 else a, x)


def from_behind(block, axis, distance):
    devices = range(lax.axis_size(axis))
    route = [(i - distance, i) for i in devices if i - distance in devices]
    return lax.ppermute(block, axis, route)


def carried_in(x, axis, combine, identity, reverse):
    length, here = lax.axis_size(axis), lax.axis_index(axis)
    everything = jax.tree.map(lambda part: lax.all_gather(part, axis), x)
    start = jax.tree.map(
        lambda part, zero: jnp.broadcast_to(jnp.asarray(zero, part.dtype), part.shape), x, identity
    )

    def hop(k, before):
        at = length - 1 - k if reverse else k
        reached = at > here if reverse else at < here
        new = combine(before, jax.tree.map(lambda part: part[at], everything))
        return jax.tree.map(lambda a, b: jnp.where(reached, a, b), new, before)

    return lax.fori_loop(0, length, hop, start)


def scattered(product, span, axis):
    everything = product(jnp.int32(0), lax.axis_size(axis) * span)
    own = lax.psum_scatter(everything.astype(jnp.bfloat16), axis, scatter_dimension=0, tiled=True)
    return own.astype(jnp.float32)


def unit_inverse(lower):
    size = lower.shape[-1]
    inverse = jnp.eye(size, dtype=jnp.float32) - lower
    power = jnp.matmul(lower, lower, precision=highest)
    span = 2
    while span < size:
        inverse = inverse + jnp.matmul(inverse, power, precision=highest)
        power = jnp.matmul(power, power, precision=highest)
        span = span * 2
    return inverse


def make_terms(query, keys, values, beta, rate_col):
    size = query.shape[-2]
    steps = jnp.arange(1, size + 1).astype(jnp.float32)
    cumulative = -rate_col * steps
    lower_mask = jnp.tril(jnp.ones((size, size), bool))
    strict_mask = jnp.tril(jnp.ones((size, size), bool), -1)
    decay = jnp.where(lower_mask, jnp.exp(cumulative[..., :, None] - cumulative[..., None, :]), 0.0)
    weighted = keys * beta[..., None]
    lower = jnp.where(
        strict_mask,
        jnp.einsum("...cd,...sd->...cs", weighted, keys, precision=highest) * decay,
        0.0,
    )
    inverse = unit_inverse(lower)
    update = jnp.einsum("...cs,...sv->...cv", inverse, values * beta[..., None], precision=highest)
    erase = jnp.einsum(
        "...cs,...sd->...cd", inverse, weighted * jnp.exp(cumulative)[..., None], precision=highest
    )
    scores = jnp.einsum("...cd,...sd->...cs", query, keys, precision=highest) * decay
    query_decayed = query * jnp.exp(cumulative)[..., None]
    final = cumulative[..., -1:]
    keys_decayed = keys * jnp.exp(final - cumulative)[..., None]
    return (query_decayed, keys_decayed, update, erase, scores, jnp.exp(final))


def apply_block(state, terms):
    query_decayed, keys_decayed, update, erase, scores, kept = terms
    fresh = update - jnp.einsum("...cd,...dv->...cv", erase, state, precision=highest)
    output = jnp.einsum("...cd,...dv->...cv", query_decayed, state, precision=highest)
    output = output + jnp.einsum("...cs,...sv->...cv", scores, fresh, precision=highest)
    state = state * kept[..., None] + jnp.einsum(
        "...cd,...cv->...dv", keys_decayed, fresh, precision=highest
    )
    return (state, output)


def causal_conv(pre, conv_taps, history):
    width = conv_taps.shape[0]
    extended = jnp.concatenate([history, pre], axis=0).astype(jnp.float32)
    length = pre.shape[0]
    total = jnp.zeros(pre.shape, jnp.float32)
    for tap in range(width):
        total = total + extended[tap : tap + length] * conv_taps[tap].astype(jnp.float32)
    return total


def rms_scale(values_in, gain):
    values = values_in.astype(jnp.float32)
    scaled = values * lax.rsqrt(jnp.mean(values * values, axis=-1, keepdims=True) + epsilon)
    return (scaled * gain).astype(jnp.bfloat16)


def l2_normalize(array):
    return array * lax.rsqrt(jnp.sum(array * array, axis=-1, keepdims=True) + epsilon)


def finish(outputs, out_gain, gate_pre):
    normed = (
        outputs
        * lax.rsqrt(jnp.mean(outputs * outputs, axis=-1, keepdims=True) + out_epsilon)
        * out_gain
    )
    gate = jax.nn.silu(gate_pre.astype(jnp.float32)).reshape(outputs.shape)
    return (normed * gate).astype(jnp.bfloat16).reshape(outputs.shape[0], outputs.shape[1], -1)


def compose(earlier, later):
    first_map, first_shift = earlier
    second_map, second_shift = later
    joined_map = jnp.einsum("shde,shef->shdf", second_map, first_map, precision=highest)
    joined_shift = (
        jnp.einsum("shde,shev->shdv", second_map, first_shift, precision=highest) + second_shift
    )
    return (joined_map, joined_shift)


def body(
    tokens,
    in_gain,
    w_query,
    w_key,
    w_value,
    w_gate,
    w_beta,
    conv_query,
    conv_key,
    conv_value,
    decay_rate,
    out_gain,
    w_out,
):
    rows = tokens.shape[0]
    seq_count = tokens.shape[1]
    width = tokens.shape[2]
    head_width = w_query.shape[1]
    local_heads = w_beta.shape[1]
    depth = head_width // local_heads
    normed = rms_scale(tokens, in_gain)
    full_query, full_key, full_value, full_gate, full_beta = (
        lax.all_gather(w_query, "sp", axis=0, tiled=True),
        lax.all_gather(w_key, "sp", axis=0, tiled=True),
        lax.all_gather(w_value, "sp", axis=0, tiled=True),
        lax.all_gather(w_gate, "sp", axis=0, tiled=True),
        lax.all_gather(w_beta, "sp", axis=0, tiled=True),
    )
    full_out = lax.all_gather(w_out, "sp", axis=1, tiled=True)

    def project(piece, start):
        flat = piece.reshape(-1, width)
        parts = [
            jnp.dot(flat, weight, preferred_element_type=jnp.float32).astype(jnp.bfloat16)
            for weight in (full_query, full_key, full_value, full_gate, full_beta)
        ]
        return jnp.concatenate(parts, axis=1).reshape(piece.shape[0], seq_count, -1)

    projected = on_whole(normed, "tp", 0, project)
    span = projected.shape[0]
    mixed_pre = projected[:, :, : 3 * head_width]
    gate_pre = projected[:, :, 3 * head_width : 4 * head_width]
    beta_pre = projected[:, :, 4 * head_width :]
    taps = conv_query.shape[0]
    history = from_behind(for_sending(mixed_pre[span - taps + 1 :]), "sp", 1)
    conv_taps = jnp.concatenate([conv_query, conv_key, conv_value], axis=1)
    convolved = jax.nn.silu(causal_conv(mixed_pre, conv_taps, history))

    def split_heads(array):
        return array.reshape(span, seq_count, local_heads, depth)

    query = l2_normalize(split_heads(convolved[:, :, :head_width])) * depth ** (-0.5)
    keys = l2_normalize(split_heads(convolved[:, :, head_width : 2 * head_width]))
    values = split_heads(convolved[:, :, 2 * head_width :])
    total_tokens = span * lax.axis_size("sp")
    beta = jax.nn.sigmoid(beta_pre.astype(jnp.float32) + math.log(depth / (4.0 * total_tokens)))
    rate_col = (decay_rate / total_tokens)[:, None]
    blocks = span // BLOCK

    def to_blocks(array):
        return jnp.moveaxis(array.reshape(blocks, BLOCK, seq_count, local_heads, depth), 1, 3)

    beta_blocks = jnp.moveaxis(beta.reshape(blocks, BLOCK, seq_count, local_heads), 1, 3)
    query_decayed, keys_decayed, update, erase, scores, kept = make_terms(
        to_blocks(query), to_blocks(keys), to_blocks(values), beta_blocks, rate_col
    )
    identity = jnp.broadcast_to(
        jnp.eye(depth, dtype=jnp.float32), (seq_count, local_heads, depth, depth)
    )
    zeros = jnp.zeros((seq_count, local_heads, depth, depth), jnp.float32)
    transfer = identity
    offset = zeros
    local_outputs = []
    readouts = []
    for index in range(blocks):
        block_terms = (
            query_decayed[index],
            keys_decayed[index],
            update[index],
            erase[index],
            scores[index],
            kept,
        )
        offset_next, output = apply_block(offset, block_terms)
        local_outputs.append(output)
        reach = query_decayed[index] - jnp.einsum(
            "shct,shtd->shcd", scores[index], erase[index], precision=highest
        )
        readouts.append(jnp.einsum("shcd,shde->shce", reach, transfer, precision=highest))
        erased = jnp.einsum("shcd,shde->shce", erase[index], transfer, precision=highest)
        transfer = transfer * kept[..., None] - jnp.einsum(
            "shcd,shce->shde", keys_decayed[index], erased, precision=highest
        )
        offset = offset_next
    prefix = carried_in(
        (for_sending(transfer), for_sending(offset)), "sp", compose, (identity, zeros), False
    )
    incoming = prefix[1]
    outputs = jnp.stack(local_outputs) + jnp.einsum(
        "nshcd,shdv->nshcv", jnp.stack(readouts), incoming, precision=highest
    )
    outputs = jnp.moveaxis(outputs, 3, 1).reshape(span, seq_count, local_heads, depth)
    gated = finish(outputs, out_gain, gate_pre)

    def head_term(start, count_rows):
        block = lax.dynamic_slice_in_dim(gated, start, count_rows, 0)
        flat = block.reshape(-1, head_width)
        return jnp.dot(flat, full_out, preferred_element_type=jnp.float32).reshape(
            count_rows, seq_count, -1
        )

    summed = scattered(head_term, rows, "tp")
    return summed.astype(jnp.bfloat16)


def solution(mesh):
    placed = (
        P(("sp", "tp"), None, None),
        P(),
        P("sp", "tp"),
        P("sp", "tp"),
        P("sp", "tp"),
        P("sp", "tp"),
        P("sp", "tp"),
        P(None, "tp"),
        P(None, "tp"),
        P(None, "tp"),
        P("tp"),
        P(),
        P("tp", "sp"),
    )
    return jax.shard_map(
        body, mesh=mesh, in_specs=placed, out_specs=P(("sp", "tp"), None, None), check_vma=False
    )
```

profile of v0, /device:TPU:0, one launch (start us, length us, event | category | flops | bytes accessed | tf_op | source)
XLA Modules:
  0.0 574.6 jit_solution(17827040287720468759)
XLA Ops:
  11.0 42.7 %all-gather.2 = bf16[16,64,4]{1,2,0:T(4,128)(2,1)S(1)} all-gather(bf16[1,64,4]{1,2,0:T(4,128)(2,1)} %bitcast.190), channel_id=1, replica_groups=mesh['sp'=16,'tp'=2] {'sp'}, dimensions={0}, use_global_device_ids=true | all-gather | bytes 8704 | tf_op jit(solution)/shard_map/all_gather | solution.py:168
  56.4 2.4 all_gather.33
  59.9 8.0 %all-gather.11.cloned.1.call-done = bf16[1024,512]{1,0:T(8,128)(2,1)} async-done(((bf16[64,512]{1,0:T(8,128)(2,1)}), bf16[1024,512]{1,0:T(8,128)(2,1)}) %all-gather.11.cloned.1.call-update) | async-done | bytes 1048592 | tf_op jit(solution)/shard_map/all_gather | solution.py:164
  69.7 54.9 %all-gather.13.cloned.1.call-done = bf16[1024,512]{1,0:T(8,128)(2,1)} async-done(((bf16[64,512]{1,0:T(8,128)(2,1)}), bf16[1024,512]{1,0:T(8,128)(2,1)}) %all-gather.13.cloned.1.call-update) | async-done | bytes 1048592 | tf_op jit(solution)/shard_map/all_gather | solution.py:165
  126.5 54.9 %all-gather.15.cloned.1.call-done = bf16[1024,512]{1,0:T(8,128)(2,1)} async-done(((bf16[64,512]{1,0:T(8,128)(2,1)}), bf16[1024,512]{1,0:T(8,128)(2,1)}) %all-gather.15.cloned.1.call-update) | async-done | bytes 1048592 | tf_op jit(solution)/shard_map/all_gather | solution.py:166
  183.2 54.8 %all-gather.17.cloned.1.call-done = bf16[1024,512]{1,0:T(8,128)(2,1)} async-done(((bf16[64,512]{1,0:T(8,128)(2,1)}), bf16[1024,512]{1,0:T(8,128)(2,1)}) %all-gather.17.cloned.1.call-update) | async-done | bytes 1048592 | tf_op jit(solution)/shard_map/all_gather | solution.py:167
  240.3 3.4 collective-permute-start
  246.1 2.7 divide_multiply_fusion
  267.3 1.9 convolution_subtract_fusion.1
  270.2 2.8 fusion.11
  273.3 2.5 reshape.279
  275.7 2.6 fusion.38
  284.6 2.8 fusion.12
  288.5 2.5 mul.263
  290.9 2.3 reduce_sum.37
  295.8 2.5 reshape.277
  299.8 3.0 convolution_multiply_fusion.1
  310.7 75.2 %all-gather.21.cloned.1.call-done = bf16[64,4,128,128]{3,2,1,0:T(8,128)(2,1)} async-done(((bf16[4,4,128,128]{3,2,1,0:T(8,128)(2,1)}), bf16[64,4,128,128]{3,2,1,0:T(8,128)(2,1)}) %all-gather.21.cloned.1.call-update) | async-done | bytes 8388624 | tf_op jit(solution)/shard_map/all_gather | solution.py:33
  386.0 113.1 %all-gather.23.cloned.1.call-done = bf16[64,4,128,128]{3,2,1,0:T(8,128)(2,1)} async-done(((bf16[4,4,128,128]{3,2,1,0:T(8,128)(2,1)}), bf16[64,4,128,128]{3,2,1,0:T(8,128)(2,1)}) %all-gather.23.cloned.1.call-update) | async-done | bytes 8388624 | tf_op jit(solution)/shard_map/all_gather | solution.py:33
  499.0 25.9 %while.14 = (s32[]{:T(128)}, bf16[4,4,128,128]{3,2,1,0:T(8,128)(2,1)S(1)}, s32[]{:T(128)}, bf16[16,4,4,128,128]{4,3,2,1,0:T(8,128)(2,1)}, bf16[16,4,4,128,128]{4,3,2,1,0:T(8,128)(2,1)}, /*index=5*/s32[]{:T(128)}, s32[]{:T(128)}) while((s32[]{:T(128)}, bf16[4,4,128,128]{3,2,1,0:T(8,128)(2,1)S(1)}, s32[]{:T(128)}, ...), condition=%wide.region_4.5_spmd.clone, body=%wide.region_3.4_spmd.clone.sunk | while | flops 68157440 | bytes 3672679 | solution.py:44
  527.6 27.6 %all-gather.19.cloned.1.call-done = bf16[512,1024]{0,1:T(8,128)(2,1)} async-done(((bf16[512,64]{0,1:T(8,128)(2,1)}), bf16[512,1024]{0,1:T(8,128)(2,1)}) %all-gather.19.cloned.1.call-update) | async-done | bytes 1048592 | tf_op jit(solution)/shard_map/all_gather | solution.py:170
  555.2 2.8 convolution_convert_fusion
  558.0 7.2 %reduce-scatter.2.cloned.1.call-done = bf16[48,4,1024]{2,0,1:T(8,128)(2,1)} async-done(((bf16[96,4,1024]{2,0,1:T(8,128)(2,1)}), bf16[48,4,1024]{2,0,1:T(8,128)(2,1)}) %reduce-scatter.2.cloned.1.call-update) | async-done | bytes 393232 | tf_op jit(solution)/shard_map/reduce_scatter | solution.py:49
  565.2 2.0 copy.149
  (185 shorter events, 84.5 us)
Async XLA Ops:
  6.5 281.9 %copy-start = (f32[128]{0:T(128)S(1)}, f32[128]{0:T(128)}, u32[]{:S(2)}) copy-start(f32[128]{0:T(128)} %param.26) | copy-start | bytes 1540
  6.5 61.4 %all-gather.11.cloned.1.call-start = ((), (), s32[]{:S(2)}) async-start(), calls=%async_computation.1 | async-start | bytes 1114112 | tf_op jit(solution)/shard_map/all_gather | solution.py:164
  7.3 117.4 %all-gather.13.cloned.1.call-start = ((), (), s32[]{:S(2)}) async-start(), calls=%async_computation.2 | async-start | bytes 1114112 | tf_op jit(solution)/shard_map/all_gather | solution.py:165
  8.0 173.4 %all-gather.15.cloned.1.call-start = ((), (), s32[]{:S(2)}) async-start(), calls=%async_computation.3 | async-start | bytes 1114112 | tf_op jit(solution)/shard_map/all_gather | solution.py:166
  8.7 229.2 %all-gather.17.cloned.1.call-start = ((), (), s32[]{:S(2)}) async-start(), calls=%async_computation.4 | async-start | bytes 1114112 | tf_op jit(solution)/shard_map/all_gather | solution.py:167
  9.3 376.6 %all-gather.21.cloned.1.call-start = ((), (), s32[]{:S(2)}) async-start(), calls=%async_computation.7 | async-start | bytes 8912896 | tf_op jit(solution)/shard_map/all_gather | solution.py:33
  55.1 4.4 copy-start.19
  55.1 4.4 copy-start.20
  59.9 192.7 %copy-start.18 = (f32[4,32,32]{2,1,0:T(8,128)}, f32[4,32,32]{2,1,0:T(8,128)S(1)}, u32[]{:S(2)}) copy-start(f32[4,32,32]{2,1,0:T(8,128)S(1)} %exponential_select_fusion) | copy-start | bytes 49156
  240.3 5.8 %copy-start.11 = (bf16[96,4,2052]{2,1,0:T(4,128)(2,1)}, bf16[96,4,2052]{2,1,0:T(4,128)(2,1)S(1)}, u32[]{:S(2)}) copy-start(bf16[96,4,2052]{2,1,0:T(4,128)(2,1)S(1)} %reshape.262) | copy-start | bytes 4727812
  240.3 5.0 collective-permute-start
  252.6 17.6 %copy-start.9 = (f32[3,4,4,32,128]{4,3,2,1,0:T(8,128)}, f32[3,4,4,32,128]{4,3,2,1,0:T(8,128)S(1)}, u32[]{:S(2)}) copy-start(f32[3,4,4,32,128]{4,3,2,1,0:T(8,128)S(1)} %bitcast_multiply_fusion.2) | copy-start | bytes 2359300
  262.0 5.3 copy-start.8
  263.4 5.8 %copy-start.5 = (f32[3,4,4,32,128]{4,3,2,1,0:T(8,128)}, f32[3,4,4,32,128]{4,3,2,1,0:T(8,128)S(1)}, u32[]{:S(2)}) copy-start(f32[3,4,4,32,128]{4,3,2,1,0:T(8,128)S(1)} %fusion.32) | copy-start | bytes 2359300
  269.2 6.6 %copy-start.1 = (f32[4,4,128,128]{3,2,1,0:T(8,128)}, f32[4,4,128,128]{3,2,1,0:T(8,128)S(1)}, u32[]{:S(2)}) copy-start(f32[4,4,128,128]{3,2,1,0:T(8,128)S(1)} %convolution_subtract_fusion.1) | copy-start | bytes 3145732
  273.0 226.0 %all-gather.23.cloned.1.call-start = ((), (), s32[]{:S(2)}) async-start(), calls=%async_computation.8 | async-start | bytes 8912896 | tf_op jit(solution)/shard_map/all_gather | solution.py:33
  278.7 4.8 copy-start.14
  280.6 4.0 copy-start.3
  287.4 267.8 %all-gather.19.cloned.1.call-start = ((), (), s32[]{:S(2)}) async-start(), calls=%async_computation.5 | async-start | bytes 1114112 | tf_op jit(solution)/shard_map/all_gather | solution.py:170
  288.1 277.1 %reduce-scatter.2.cloned.1.call-start = ((), (), s32[]{:S(2)}) async-start(), calls=%async_computation.6 | async-start | bytes 1179648 | tf_op jit(solution)/shard_map/reduce_scatter | solution.py:49
  298.2 5.0 copy-start.7
  304.4 4.1 copy-start.2
  305.4 4.1 copy-start.15
  526.4 28.8 %slice-start = ((bf16[96,4,2052]{2,1,0:T(4,128)(2,1)}), bf16[96,4,512]{2,1,0:T(4,128)(2,1)S(1)}, s32[]{:S(2)}) async-start(bf16[96,4,2052]{2,1,0:T(4,128)(2,1)} %copy-done.11), calls=%async_computation.9 | async-start | bytes 786432 | tf_op jit(solution)/shard_map/slice | solution.py:183
  (7 other events, 20.2 us)
Sparse Core Ops, SparseCore 0:
  10.1 57.7 all-gather.10
  70.7 53.9 all-gather.12
  127.4 53.9 all-gather.14
  184.0 53.9 all-gather.16
  273.1 112.7 all-gather.20
  388.6 110.4 all-gather.22
  501.8 53.3 all-gather.18
  558.1 7.0 reduce-scatter.1
where the time goes:
time: 580 us; the launch traced here: 575 us
  waiting for transfers between devices  400 us (69%)
  matrix products  78 us (13%)
  blocking collectives  45.1 us (8%)
  local copies, waits for them, and re-layouts  18.1 us (3%)
  between operations  14.7 us (3%)
  other arithmetic  13.7 us (2%)
    all_gather x2, waiting for transfers between devices, carried_in(): everything = jax.tree.map(lambda part: lax.all_gather(part, axis), x)  188 us
    all_gather x1, waiting for transfers between devices, body(): lax.all_gather(w_value, 'sp', axis=0, tiled=True)  54.9 us
    all_gather x1, waiting for transfers between devices, body(): lax.all_gather(w_key, 'sp', axis=0, tiled=True)  54.9 us
    all_gather x1, waiting for transfers between devices, body(): lax.all_gather(w_gate, 'sp', axis=0, tiled=True)  54.8 us
    all_gather x1, blocking collectives, body(): lax.all_gather(w_beta, 'sp', axis=0, tiled=True)  42.7 us
    all_gather x1, waiting for transfers between devices, body(): full_out = lax.all_gather(w_out, 'sp', axis=1, tiled=True)  27.6 us
    dot_general x16, matrix products, compose(): jnp.einsum('shde,shev->shdv', second_map, first_shift, precision=highest)  24.4 us
  transfers between devices with their start and end apart: 9, of which 9 were waited for; matrix products, arithmetic and copies ran while one was open for 13% of the time, Pallas kernels for 0%

commit v1 on v0

v1 whole, which is shorter than its diff:
```python
import functools
import math

import jax
import jax.numpy as jnp
from jax import lax
from jax.experimental import pallas as pl
from jax.experimental.pallas import tpu as pltpu
from jax.sharding import PartitionSpec as P

PAD = 16
LANES = 128
epsilon = 1e-06
out_epsilon = 1e-10
f32 = jnp.float32
bf16 = jnp.bfloat16
NN, NT, TN = ((1,), (0,)), ((1,), (1,)), ((0,), (0,))


def dot(a, b, dims=NN):
    return lax.dot_general(
        a.astype(bf16), b.astype(bf16), (dims, ((), ())), preferred_element_type=f32
    )


def rms_scale(values_in, gain):
    values = values_in.astype(f32)
    scaled = values * lax.rsqrt(jnp.mean(values * values, axis=-1, keepdims=True) + epsilon)
    return (scaled * gain).astype(bf16)


def l2_normalize(array):
    return array * lax.rsqrt(jnp.sum(array * array, axis=-1, keepdims=True) + epsilon)


def unit_inverse(lower, row, col):
    size = lower.shape[0]
    near = ((row >> 1) == (col >> 1)) & (row != col)
    inverse = jnp.where(row == col, 1.0, 0.0) - jnp.where(near, lower, 0.0)
    level = 1
    while (1 << level) < size:
        mask = ((row >> (level + 1)) == (col >> (level + 1))) & ((row >> level) != (col >> level))
        cross = jnp.where(mask, lower, 0.0)
        inverse = inverse - dot(inverse, dot(cross, inverse))
        level += 1
    return inverse


def pair_terms(block, beta, taps, rate, depth):
    width = taps[0].shape[0]
    size = beta.shape[0]

    def conv(part):
        x = block[part].astype(f32)
        total = x * taps[part][width - 1 : width]
        for back in range(1, width):
            total = total + pltpu.roll(x, back, 0) * taps[part][width - 1 - back : width - back]
        total = total[PAD:]
        return total * jax.nn.sigmoid(total)

    query = l2_normalize(conv(0)) * depth ** (-0.5)
    keys = l2_normalize(conv(1))
    values = conv(2)
    row = lax.broadcasted_iota(jnp.int32, (size, size), 0)
    col = lax.broadcasted_iota(jnp.int32, (size, size), 1)
    decay = jnp.exp(-rate * jnp.maximum(row - col, 0).astype(f32))
    step = lax.broadcasted_iota(jnp.int32, (size, 1), 0).astype(f32)
    kept = jnp.exp(-rate * (step + 1.0))
    rest = jnp.exp(-rate * (size - 1.0 - step))
    weighted = keys * beta
    products = dot(jnp.concatenate([weighted, query], axis=0), keys, NT)
    lower = jnp.where(row > col, products[:size] * decay, 0.0)
    scores = jnp.where(row >= col, products[size:] * decay, 0.0)
    inverse = unit_inverse(lower, row, col)
    both = dot(inverse, jnp.concatenate([values * beta, weighted * kept], axis=1))
    seen = dot(scores, both)
    moved = dot(keys * rest, both, TN)
    return moved, query * kept - seen[:, depth:], seen[:, :depth]


def terms_kernel(heads, depth, shift, pre_ref, taps_ref, rate_ref, map_ref, read_ref, local_ref):
    head_width = heads * depth
    beta = jax.nn.sigmoid(pre_ref[0, PAD:, 4 * head_width :].astype(f32) + shift)
    for head in range(heads):
        places = [pl.ds(part * head_width + head * depth, depth) for part in range(3)]
        moved, read, local = pair_terms(
            [pre_ref[0, :, place] for place in places],
            beta[:, head : head + 1],
            [taps_ref[:, place] for place in places],
            rate_ref[head],
            depth,
        )
        map_ref[0, head] = moved.astype(bf16)
        read_ref[0, head] = read.astype(bf16)
        local_ref[0, head] = local


def chain_kernel(depth, kept_ref, map_ref, state_ref):
    state = jnp.zeros((depth, depth), f32)
    for index in range(map_ref.shape[0]):
        state_ref[index] = state.astype(bf16)
        state = (
            state * kept_ref[0]
            + map_ref[index, :, :depth].astype(f32)
            - dot(map_ref[index, :, depth:], state)
        )


def finish_kernel(heads, depth, read_ref, local_ref, state_ref, pre_ref, gain_ref, gated_ref):
    for head in range(heads):
        out = local_ref[0, head] + dot(read_ref[0, head], state_ref[0, head])
        out = out * lax.rsqrt(jnp.mean(out * out, axis=-1, keepdims=True) + out_epsilon)
        place = pl.ds(head * depth, depth)
        gate = pre_ref[0, PAD:, place].astype(f32)
        gate = gate * jax.nn.sigmoid(gate)
        gated_ref[0, :, place] = (out * gain_ref[...] * gate).astype(bf16)


def incoming_states(maps, kept):
    pairs, depth, _ = maps.shape
    length, here = lax.axis_size("sp"), lax.axis_index("sp")
    if pairs == length:
        mine = lax.all_to_all(maps, "sp", 0, 0, tiled=True)
        states = pl.pallas_call(
            functools.partial(chain_kernel, depth),
            out_shape=jax.ShapeDtypeStruct((length, depth, depth), bf16),
            in_specs=[
                pl.BlockSpec(memory_space=pltpu.SMEM),
                pl.BlockSpec(memory_space=pltpu.VMEM),
            ],
            out_specs=pl.BlockSpec(memory_space=pltpu.VMEM),
        )(lax.dynamic_slice_in_dim(kept, here, 1, 0), mine)
        return lax.all_to_all(states, "sp", 0, 0, tiled=True)
    everything = lax.all_gather(maps, "sp")

    def hop(index, state):
        moved = everything[index].astype(f32)
        erased = jnp.einsum(
            "pde,pev->pdv",
            moved[:, :, depth:].astype(bf16),
            state.astype(bf16),
            preferred_element_type=f32,
        )
        new = state * kept[:, None, None] + moved[:, :, :depth] - erased
        return jnp.where(index < here, new, state)

    state = lax.fori_loop(0, length, hop, jnp.zeros((pairs, depth, depth), f32))
    return state.astype(bf16)


def body(
    tokens,
    in_gain,
    w_query,
    w_key,
    w_value,
    w_gate,
    w_beta,
    conv_query,
    conv_key,
    conv_value,
    decay_rate,
    out_gain,
    w_out,
):
    seqs, width = tokens.shape[1], tokens.shape[2]
    head_width = w_query.shape[1]
    heads = w_beta.shape[1]
    depth = head_width // heads
    taps = conv_query.shape[0]
    length = lax.axis_size("sp")

    beta_pad = jnp.pad(w_beta, ((0, 0), (0, LANES - heads)))
    packed = jnp.concatenate([w_query, w_key, w_value, w_gate, beta_pad], axis=1)
    weights = lax.all_gather(packed, "sp", axis=0, tiled=True)
    full_out = lax.all_gather(w_out.T, "sp", axis=0, tiled=True)

    normed = jnp.swapaxes(rms_scale(tokens, in_gain), 0, 1)
    normed = lax.all_gather(normed, "tp", axis=1, tiled=True)
    span = normed.shape[1]
    history = lax.ppermute(
        normed[:, span - taps + 1 :], "sp", [(i, i + 1) for i in range(length - 1)]
    )
    filler = jnp.zeros((seqs, PAD - taps + 1, width), bf16)
    extended = jnp.concatenate([filler, history, normed], axis=1)
    rows = PAD + span
    pre = jnp.dot(
        extended.reshape(-1, width), weights, preferred_element_type=f32
    ).astype(bf16)
    pre = pre.reshape(seqs, rows, -1)

    total_tokens = span * length
    rate = decay_rate / total_tokens
    shift = math.log(depth / (4.0 * total_tokens))
    conv_taps = jnp.concatenate([conv_query, conv_key, conv_value], axis=1).astype(f32)

    def per_seq(*shape):
        return pl.BlockSpec((1,) + shape, lambda s: (s,) + (0,) * len(shape))

    maps, reads, locals_ = pl.pallas_call(
        functools.partial(terms_kernel, heads, depth, shift),
        grid=(seqs,),
        in_specs=[
            per_seq(rows, pre.shape[2]),
            pl.BlockSpec(conv_taps.shape, lambda s: (0, 0)),
            pl.BlockSpec(memory_space=pltpu.SMEM),
        ],
        out_specs=[
            per_seq(heads, depth, 2 * depth),
            per_seq(heads, span, depth),
            per_seq(heads, span, depth),
        ],
        out_shape=[
            jax.ShapeDtypeStruct((seqs, heads, depth, 2 * depth), bf16),
            jax.ShapeDtypeStruct((seqs, heads, span, depth), bf16),
            jax.ShapeDtypeStruct((seqs, heads, span, depth), f32),
        ],
    )(pre, conv_taps, rate)

    kept = jnp.tile(jnp.exp(-rate * span), seqs)
    states = incoming_states(maps.reshape(seqs * heads, depth, 2 * depth), kept)
    gated = pl.pallas_call(
        functools.partial(finish_kernel, heads, depth),
        grid=(seqs,),
        in_specs=[
            per_seq(heads, span, depth),
            per_seq(heads, span, depth),
            per_seq(heads, depth, depth),
            pl.BlockSpec((1, rows, head_width), lambda s: (s, 0, 3)),
            pl.BlockSpec((1, depth), lambda s: (0, 0)),
        ],
        out_specs=per_seq(span, head_width),
        out_shape=jax.ShapeDtypeStruct((seqs, span, head_width), bf16),
    )(reads, locals_, states.reshape(seqs, heads, depth, depth), pre, out_gain[None])

    mixed = lax.dot_general(
        gated, full_out, (((2,), (1,)), ((), ())), preferred_element_type=f32
    ).astype(bf16)
    mixed = lax.psum_scatter(mixed, "tp", scatter_dimension=1, tiled=True)
    return jnp.swapaxes(mixed, 0, 1)


def solution(mesh):
    placed = (
        P(("sp", "tp"), None, None),
        P(),
        P("sp", "tp"),
        P("sp", "tp"),
        P("sp", "tp"),
        P("sp", "tp"),
        P("sp", "tp"),
        P(None, "tp"),
        P(None, "tp"),
        P(None, "tp"),
        P("tp"),
        P(),
        P("tp", "sp"),
    )
    return jax.shard_map(
        body, mesh=mesh, in_specs=placed, out_specs=P(("sp", "tp"), None, None), check_vma=False
    )
```

time: 580 us -> 219 us (0.38)
  waiting for transfers between devices: 400 us -> 108 us
  matrix products: 78 us -> 8.78 us
  Pallas kernels: 0 us -> 41.7 us
  blocking collectives: 45.1 us -> 24.9 us
  other arithmetic: 13.7 us -> 3.89 us
  local copies, waits for them, and re-layouts: 18.1 us -> 8.73 us
    all_gather x7 -> x2, waiting for transfers between devices: 389 us -> 76.6 us  [the longest x1 68.6 us: body(): weights = lax.all_gather(packed, 'sp', axis=0, tiled=True)]
    dot_general x59 -> x2, matrix products: 78 us -> 8.78 us  [the longest x1 5.88 us: body(): jnp.dot(extended.reshape(-1, width), weights, preferred_element_type=f32)]
    all_gather x2 -> x1, blocking collectives: 45.1 us -> 2.51 us  [body(): normed = lax.all_gather(normed, 'tp', axis=1, tiled=True)]
    pallas_call x0 -> x3, Pallas kernels: none -> 41.7 us  [the longest x1 32.9 us: body(): pl.pallas_call(functools.partial(terms_kernel, heads, depth, shift), grid...]
    all_to_all x0 -> x1, waiting for transfers between devices: none -> 23.2 us  [incoming_states(): mine = lax.all_to_all(maps, 'sp', 0, 0, tiled=True)]
    all_to_all x0 -> x1, blocking collectives: none -> 22.4 us  [incoming_states(): return lax.all_to_all(states, 'sp', 0, 0, tiled=True)]
    mul x5 -> x0, other arithmetic: 6.39 us -> none  [the longest x1 2.7 us: body(): convolved = jax.nn.silu(causal_conv(mixed_pre, conv_taps, history))]
  transfers between devices with their start and end apart: 9 -> 5, of which waited for: 9 -> 5; matrix products, arithmetic and copies ran while one was open for 13% -> 2% of each run, Pallas kernels for 0% -> 4%
where the time goes in v1:
time: 219 us
  waiting for transfers between devices  108 us (49%)
  Pallas kernels  41.7 us (19%)
  blocking collectives  24.9 us (11%)
  between operations  13.2 us (6%)
  starting transfers between devices  9.42 us (4%)
  matrix products  8.78 us (4%)
  local copies, waits for them, and re-layouts  8.73 us (4%)
  other arithmetic  3.89 us (2%)
    all_gather x1, waiting for transfers between devices, body(): weights = lax.all_gather(packed, 'sp', axis=0, tiled=True)  68.6 us
    pallas_call x1, Pallas kernels, body(): pl.pallas_call(functools.partial(terms_kernel, heads, depth, shift), grid...  32.9 us
    all_to_all x1, waiting for transfers between devices, incoming_states(): mine = lax.all_to_all(maps, 'sp', 0, 0, tiled=True)  23.2 us
    all_to_all x1, blocking collectives, incoming_states(): return lax.all_to_all(states, 'sp', 0, 0, tiled=True)  22.4 us
    all_gather x1, waiting for transfers between devices, body(): full_out = lax.all_gather(w_out.T, 'sp', axis=0, tiled=True)  7.93 us
    reduce_scatter x1, waiting for transfers between devices, body(): mixed = lax.psum_scatter(mixed, 'tp', scatter_dimension=1, tiled=True)  7.19 us
    unnamed x17, local copies, waits for them, and re-layouts  5.89 us
    dot_general x1, matrix products, body(): jnp.dot(extended.reshape(-1, width), weights, preferred_element_type=f32)  5.88 us
  transfers between devices with their start and end apart: 5, of which 5 were waited for; matrix products, arithmetic and copies ran while one was open for 2% of the time, Pallas kernels for 4%

profile of v1, /device:TPU:0, one launch (start us, length us, event | category | flops | bytes accessed | tf_op | source)
XLA Modules:
  0.0 218.6 jit_solution(6438311070009536752)
XLA Ops:
  6.6 0.9 constant_dynamic-update-slice_fusion.3
  7.4 0.8 copy.19
  8.2 0.8 constant_dynamic-update-slice_fusion.2
  9.1 0.8 constant_dynamic-update-slice_fusion.1
  9.9 0.8 constant_dynamic-update-slice_fusion
  10.8 0.7 copy-done.1
  11.5 1.2 fusion.1
  12.7 1.2 fusion.4
  13.9 2.5 %all_gather.9 = bf16[4,96,1024]{2,1,0:T(8,128)(2,1)S(1)} all-gather(bf16[4,48,1024]{2,1,0:T(8,128)(2,1)S(1)} %fusion.4), channel_id=1, replica_groups=mesh['sp'=16,'tp'=2] {'tp'}, dimensions={1}, use_global_device_ids=true | all-gather | bytes 1179648 | tf_op jit(solution)/shard_map/all_gather | solution.py:179
  16.5 4.8 %collective-permute-start = (bf16[4,3,1024]{2,1,0:T(4,128)(2,1)S(1)}, bf16[4,3,1024]{2,1,0:T(4,128)(2,1)S(1)}, u32[]{:S(2)}, u32[]{:S(2)}) collective-permute-start(bf16[4,3,1024]{2,1,0:T(4,128)(2,1)S(1)} %slice.4), channel_id=1, source_target_pairs={{0,2},{2,4},{4,6},{6,8},{8,10},{10,12},{12,14},{14,16},{16,18},{18... | collective-permute-start | bytes 73736 | tf_op jit(solution)/shard_map/ppermute | solution.py:181
  23.1 68.6 %all-gather.3.cloned.1.call-done = bf16[1024,2176]{1,0:T(8,128)(2,1)} async-done(((bf16[64,2176]{1,0:T(8,128)(2,1)}), bf16[1024,2176]{1,0:T(8,128)(2,1)}) %all-gather.3.cloned.1.call-update) | async-done | bytes 4456464 | tf_op jit(solution)/shard_map/all_gather | solution.py:175
  91.7 5.9 %convolution_convert_fusion = bf16[448,2176]{1,0:T(8,128)(2,1)} fusion(bf16[448,1024]{1,0:T(8,128)(2,1)S(1)} %bitcast.19, bf16[1024,2176]{1,0:T(8,128)(2,1)} %all-gather.3.cloned.1.call-done), kind=kOutput, calls=%fused_computation | convolution fusion | flops 1997463552 | bytes 7323648 | tf_op jit(solution)/shard_map/dot_general | solution.py:187
  97.6 32.9 %shard_map.127 = (bf16[4,4,128,256]{3,2,1,0:T(8,128)(2,1)}, bf16[4,4,96,128]{3,2,1,0:T(8,128)(2,1)}, f32[4,4,96,128]{3,2,1,0:T(8,128)}) custom-call(bf16[4,112,2176]{2,1,0:T(8,128)(2,1)} %bitcast.15, f32[4,1536]{1,0:T(4,128)} %maximum_convert_fusion.taps_ref, f32[4]{0:T(128)} %get-tuple-element.12.rate_ref), custom_call_target="tpu_custom_call" | custom-call | tf_op jit(solution)/shard_map/pallas_call | solution.py:200
  130.6 4.5 %all-to-all-start = ((bf16[16,128,256]{2,1,0:T(8,128)(2,1)}), bf16[16,128,256]{2,1,0:T(8,128)(2,1)S(1)}, u32[]{:S(2)}, u32[]{:S(2)}) async-start(bf16[16,128,256]{2,1,0:T(8,128)(2,1)} %bitcast.18), calls=%async_computation | async-start | bytes 2097152 | tf_op jit(solution)/shard_map/all_to_all | solution.py:123
  135.2 0.7 all-gather.5.cloned.1.call-update
  136.7 23.2 %all-to-all-done.map_ref = bf16[16,128,256]{2,1,0:T(8,128)(2,1)S(1)} async-done(((bf16[16,128,256]{2,1,0:T(8,128)(2,1)}), bf16[16,128,256]{2,1,0:T(8,128)(2,1)S(1)}, u32[]{:S(2)}, u32[]{:S(2)}) %all-to-all-start) | async-done | bytes 1048608 | tf_op jit(solution)/shard_map/all_to_all | solution.py:123
  159.9 1.0 copy-done
  160.9 4.7 %shard_map.128 = bf16[16,128,128]{2,1,0:T(8,128)(2,1)} custom-call(f32[1]{0:T(128)} %dynamic_slice.3.kept_ref, bf16[16,128,256]{2,1,0:T(8,128)(2,1)} %copy-done), custom_call_target="tpu_custom_call" | custom-call | tf_op jit(solution)/shard_map/pallas_call | solution.py:124
  165.6 22.4 %all_to_all.10 = bf16[16,128,128]{2,1,0:T(8,128)(2,1)} all-to-all(bf16[16,128,128]{2,1,0:T(8,128)(2,1)} %shard_map.128), channel_id=1, replica_groups=mesh['sp'=16,'tp'=2] {'sp'}, dimensions={0} | all-to-all | bytes 1048576 | tf_op jit(solution)/shard_map/all_to_all | solution.py:133
  187.9 4.1 %shard_map.129 = bf16[4,96,512]{2,1,0:T(8,128)(2,1)} custom-call(bf16[4,4,96,128]{3,2,1,0:T(8,128)(2,1)} %get-tuple-element.8.read_ref, f32[4,4,96,128]{3,2,1,0:T(8,128)} %get-tuple-element.9.local_ref, bf16[4,4,128,128]{3,2,1,0:T(8,128)(2,1)} %bitcast.17, bf16[4,112,2176]{2,1,0:T(8,128)(2,1)} %bitcast.16, f32[1,128]{1,0:T(1,128)} %bitcast.22), custom_call_target="tpu_custom_call" | custom-call | tf_op jit(solution)/shard_map/pallas_call | solution.py:222
  192.0 7.9 %all-gather.5.cloned.1.call-done = bf16[1024,512]{1,0:T(8,128)(2,1)} async-done(((bf16[64,512]{1,0:T(8,128)(2,1)}), bf16[1024,512]{1,0:T(8,128)(2,1)}) %all-gather.5.cloned.1.call-update) | async-done | bytes 1048592 | tf_op jit(solution)/shard_map/all_gather | solution.py:176
  199.9 2.9 %convolution_convert_fusion.1 = bf16[4,96,1024]{2,1,0:T(8,128)(2,1)} fusion(bf16[4,96,512]{2,1,0:T(8,128)(2,1)} %shard_map.129, bf16[1024,512]{1,0:T(8,128)(2,1)} %all-gather.5.cloned.1.call-done), kind=kOutput, calls=%fused_computation.1 | convolution fusion | flops 403046400 | bytes 2228224 | tf_op jit(solution)/shard_map/dot_general | solution.py:236
  202.8 7.2 %reduce-scatter.2.cloned.1.call-done = bf16[4,48,1024]{2,1,0:T(8,128)(2,1)} async-done(((bf16[4,96,1024]{2,1,0:T(8,128)(2,1)}), bf16[4,48,1024]{2,1,0:T(8,128)(2,1)}) %reduce-scatter.2.cloned.1.call-update) | async-done | bytes 393232 | tf_op jit(solution)/shard_map/reduce_scatter | solution.py:239
  210.0 2.0 copy.18
  (27 shorter events, 2.8 us)
Async XLA Ops:
  6.5 14.7 %copy-start.2 = (bf16[4,512]{1,0:T(4,128)(2,1)S(1)}, bf16[4,512]{1,0:T(4,128)(2,1)}, u32[]{:S(2)}) copy-start(bf16[4,512]{1,0:T(4,128)(2,1)} %param.22) | copy-start | bytes 12292
  6.5 14.7 %copy-start.3 = (bf16[4,512]{1,0:T(4,128)(2,1)S(1)}, bf16[4,512]{1,0:T(4,128)(2,1)}, u32[]{:S(2)}) copy-start(bf16[4,512]{1,0:T(4,128)(2,1)} %param.21) | copy-start | bytes 12292
  6.5 14.7 %copy-start.4 = (bf16[4,512]{1,0:T(4,128)(2,1)S(1)}, bf16[4,512]{1,0:T(4,128)(2,1)}, u32[]{:S(2)}) copy-start(bf16[4,512]{1,0:T(4,128)(2,1)} %param.20) | copy-start | bytes 12292
  6.5 15.3 %copy-start.5 = (f32[4]{0:T(128)S(1)}, f32[4]{0:T(128)}, u32[]{:S(2)}) copy-start(f32[4]{0:T(128)} %param.23) | copy-start | bytes 52
  6.5 85.2 %all-gather.3.cloned.1.call-start = ((), (), s32[]{:S(2)}) async-start(), calls=%async_computation.3 | async-start | bytes 4734976 | tf_op jit(solution)/shard_map/all_gather | solution.py:175
  10.8 0.7 copy-start.1
  16.5 6.3 %collective-permute-start = (bf16[4,3,1024]{2,1,0:T(4,128)(2,1)S(1)}, bf16[4,3,1024]{2,1,0:T(4,128)(2,1)S(1)}, u32[]{:S(2)}, u32[]{:S(2)}) collective-permute-start(bf16[4,3,1024]{2,1,0:T(4,128)(2,1)S(1)} %slice.4), channel_id=1, source_target_pairs={{0,2},{2,4},{4,6},{6,8},{8,10},{10,12},{12,14},{14,16},{16,18},{18... | collective-permute-start | bytes 73736 | tf_op jit(solution)/shard_map/ppermute | solution.py:181
  130.6 29.3 %all-to-all-start = ((bf16[16,128,256]{2,1,0:T(8,128)(2,1)}), bf16[16,128,256]{2,1,0:T(8,128)(2,1)S(1)}, u32[]{:S(2)}, u32[]{:S(2)}) async-start(bf16[16,128,256]{2,1,0:T(8,128)(2,1)} %bitcast.18), calls=%async_computation | async-start | bytes 2097152 | tf_op jit(solution)/shard_map/all_to_all | solution.py:123
  135.1 64.8 %all-gather.5.cloned.1.call-start = ((), (), s32[]{:S(2)}) async-start(), calls=%async_computation.4 | async-start | bytes 1114112 | tf_op jit(solution)/shard_map/all_gather | solution.py:176
  135.9 74.2 %reduce-scatter.2.cloned.1.call-start = ((), (), s32[]{:S(2)}) async-start(), calls=%async_computation.5 | async-start | bytes 1179648 | tf_op jit(solution)/shard_map/reduce_scatter | solution.py:239
  159.9 1.0 copy-start
Sparse Core Ops, SparseCore 0:
  11.6 80.0 all-gather.2
  138.7 61.1 all-gather.4
  203.0 7.0 reduce-scatter.1
